TPU v7x, 32 devices: a whole 2x2x4 slice. The times are simulated.
32 devices in a mesh: sp: 4 (over z), fs: 4 (over y, x), tp: 2 (over core).
Axes of the slice: x: 2, y: 2, z: 4, core: 2. Of those that a mesh axis runs over, the one named last changes fastest.
Arguments:
- tokens: bfloat16 [2048, 2048], P('sp', ('fs', 'tp')), may hold values from -6 to 6
- in_gain: float32 [2048], replicated, may hold values from 0.1 to 1.9
- conv_a_weight: bfloat16 [2048, 1024], P(None, ('fs', 'tp')), may hold values from -0.125 to 0.125
- conv_gate_weight: bfloat16 [2048, 1024], P(None, ('fs', 'tp')), may hold values from -0.125 to 0.125
- query_weight: bfloat16 [2048, 1024], P(None, ('fs', 'tp')), may hold values from -0.125 to 0.125
- key_weight: bfloat16 [2048, 1024], P(None, ('fs', 'tp')), may hold values from -0.125 to 0.125
- value_weight: bfloat16 [2048, 1024], P(None, ('fs', 'tp')), may hold values from -0.125 to 0.125
- conv_taps: bfloat16 [31, 1024], replicated, may hold values from -3 to 3
- conv_norm_gain: float32 [1024], replicated, may hold values from 0.1 to 1.9
- break_shift: bfloat16 [16, 2048], P(('fs', 'tp'), 'sp'), may hold values from -20 to 1
- conv_out_gain: float32 [1024], replicated, may hold values from 0.1 to 1.9
- attn_out_gain: float32 [1024], replicated, may hold values from 0.1 to 1.9
- out_weight: bfloat16 [2048, 2048], P(None, ('fs', 'tp')), may hold values from -0.125 to 0.125
Outputs:
- mixed: bfloat16 [2048, 2048], P('sp', ('fs', 'tp'))
All inputs are finite; a program needn't handle non-finite values.
Results may differ from a plain program's by a relative error of at most 0.0078.
Values may be sent and summed in bfloat16 or wider, within the bound.
A program may use at most 128 MiB of HBM per device.

v0:
```python
import jax
import jax.numpy as jnp
from jax import lax
from jax.sharding import PartitionSpec as P

HEAD_DIM = 64
epsilon = 1e-06


def passed_along(shard, axis, by):
    count = lax.axis_size(axis)
    pairs = [(i, i + by) for i in range(count) if 0 <= i + by < count]
    return lax.ppermute(shard, axis, pairs)


def per_device(
    tokens,
    in_gain,
    conv_a_weight,
    conv_gate_weight,
    query_weight,
    key_weight,
    value_weight,
    conv_taps,
    conv_norm_gain,
    break_shift,
    conv_out_gain,
    attn_out_gain,
    out_weight,
):
    rows_here = tokens.shape[0]
    model_width = in_gain.shape[0]
    channels = model_width // 2
    local_width = conv_a_weight.shape[1]
    heads_here = break_shift.shape[0]
    group_index = lax.axis_index(("fs", "tp"))
    shard_index = lax.axis_index("sp")
    stacked = jnp.concatenate(
        (conv_a_weight, conv_gate_weight, query_weight, key_weight, value_weight), axis=1
    )
    segment = lax.all_gather(tokens, ("fs", "tp"), axis=1, tiled=True)
    segment_wide = segment.astype(jnp.float32)
    scaled = (segment_wide * in_gain[None, :]).astype(jnp.bfloat16)
    totals = jnp.dot(scaled, stacked, preferred_element_type=jnp.float32)
    totals, squares = (totals, jnp.sum(segment_wide * segment_wide, axis=1))
    input_scale = lax.rsqrt(squares / model_width + epsilon)
    projected = (totals * input_scale[:, None]).astype(jnp.bfloat16)
    conv_a = projected[:, :local_width]
    conv_gate = projected[:, local_width : 2 * local_width]
    query = projected[:, 2 * local_width : 3 * local_width]
    key = projected[:, 3 * local_width : 4 * local_width]
    value = projected[:, 4 * local_width :]
    gated_input = conv_a.astype(jnp.float32) * jax.nn.sigmoid(conv_gate.astype(jnp.float32))
    reach_rows = conv_taps.shape[0] - 1
    earlier = passed_along(gated_input[rows_here - reach_rows :], "sp", 1)
    padded = jnp.concatenate((earlier, gated_input), axis=0)
    tap_values = lax.dynamic_slice_in_dim(
        conv_taps, group_index * local_width, local_width, 1
    ).astype(jnp.float32)
    conv_out = jnp.zeros((rows_here, local_width), jnp.float32)
    for offset in range(reach_rows + 1):
        conv_out = conv_out + tap_values[offset][None, :] * padded[offset : offset + rows_here]
    first_sum, second_sum = lax.psum(
        (jnp.sum(conv_out, axis=1), jnp.sum(conv_out * conv_out, axis=1)), ("fs", "tp")
    )
    row_mean = first_sum / channels
    row_spread = second_sum / channels - row_mean * row_mean
    centered = conv_out - row_mean[:, None]
    norm_gain = lax.dynamic_slice_in_dim(conv_norm_gain, group_index * local_width, local_width, 0)
    normed = centered * lax.rsqrt(row_spread + epsilon)[:, None] * norm_gain[None, :]
    conv_mixed = jax.nn.silu(normed).astype(jnp.bfloat16)
    queries = query.reshape(rows_here, heads_here, HEAD_DIM)
    query_pos = shard_index * rows_here + jnp.arange(rows_here, dtype=jnp.int32)
    score_scale = HEAD_DIM ** (-0.5)

    def attend(running, key_rows, value_rows, shift_rows, start_pos):
        outputs, behind = running
        piece_rows = key_rows.shape[0]
        key_heads = key_rows.reshape(piece_rows, heads_here, HEAD_DIM)
        value_heads = value_rows.reshape(piece_rows, heads_here, HEAD_DIM)
        scores = (
            jnp.einsum("qhd,khd->hqk", queries, key_heads, preferred_element_type=jnp.float32)
            * score_scale
        )
        scores = scores + shift_rows.astype(jnp.float32)[:, None, :]
        key_pos = start_pos + jnp.arange(piece_rows, dtype=jnp.int32)
        allowed = ((key_pos[None, :] < query_pos[:, None]) & (key_pos[None, :] >= 0))[None]
        log_fail = jnp.where(allowed, jax.nn.log_sigmoid(-scores), 0.0)
        later_sum = lax.cumsum(log_fail, axis=2, reverse=True) - log_fail + behind[:, :, None]
        weights = jnp.where(allowed, jnp.exp(jax.nn.log_sigmoid(scores) + later_sum), 0.0).astype(
            jnp.bfloat16
        )
        outputs = outputs + jnp.einsum(
            "hqk,khd->qhd", weights, value_heads, preferred_element_type=jnp.float32
        )
        return (outputs, behind + jnp.sum(log_fail, axis=2))

    start_state = (
        jnp.zeros((rows_here, heads_here, HEAD_DIM), jnp.float32),
        jnp.zeros((heads_here, rows_here), jnp.float32),
    )
    all_keys, all_values, all_shifts = (
        lax.all_gather(key, "sp", axis=0, tiled=True),
        lax.all_gather(value, "sp", axis=0, tiled=True),
        lax.all_gather(break_shift, "sp", axis=1, tiled=True),
    )
    sp_count = lax.axis_size("sp")
    grouped = 1
    while grouped * 2 * rows_here <= 1024 and sp_count % (grouped * 2) == 0:
        grouped = grouped * 2
    block_rows = grouped * rows_here
    last_block = (shard_index * rows_here + rows_here - 1) // block_rows

    def advance(counter, running):
        begin_row = (last_block - counter) * block_rows
        key_rows = lax.dynamic_slice_in_dim(all_keys, begin_row, block_rows, 0)
        value_rows = lax.dynamic_slice_in_dim(all_values, begin_row, block_rows, 0)
        shift_rows = lax.dynamic_slice_in_dim(all_shifts, begin_row, block_rows, 1)
        return attend(running, key_rows, value_rows, shift_rows, begin_row)

    outputs, behind = lax.fori_loop(0, last_block + 1, advance, start_state)
    attn_mixed = outputs.reshape(rows_here, heads_here * HEAD_DIM).astype(jnp.bfloat16)
    conv_piece = lax.all_gather(conv_mixed, ("fs", "tp"), axis=1, tiled=True)
    attn_piece = lax.all_gather(attn_mixed, ("fs", "tp"), axis=1, tiled=True)
    piece_width = conv_piece.shape[1]
    conv_wide = conv_piece.astype(jnp.float32)
    attn_wide = attn_piece.astype(jnp.float32)
    conv_scaled = (conv_wide * conv_out_gain[None, :]).astype(jnp.bfloat16)
    attn_scaled = (attn_wide * attn_out_gain[None, :]).astype(jnp.bfloat16)
    conv_rows = lax.slice_in_dim(out_weight, 0, piece_width, axis=0)
    attn_rows = lax.dynamic_slice_in_dim(out_weight, channels, piece_width, 0)
    conv_total = jnp.dot(conv_scaled, conv_rows, preferred_element_type=jnp.float32)
    attn_total = jnp.dot(attn_scaled, attn_rows, preferred_element_type=jnp.float32)
    conv_squares = jnp.sum(conv_wide * conv_wide, axis=1)
    attn_squares = jnp.sum(attn_wide * attn_wide, axis=1)
    conv_total, attn_total, conv_squares, attn_squares = (
        conv_total,
        attn_total,
        conv_squares,
        attn_squares,
    )
    conv_scale = lax.rsqrt(conv_squares / channels + epsilon)
    attn_scale = lax.rsqrt(attn_squares / channels + epsilon)
    mixed = conv_total * conv_scale[:, None] + attn_total * attn_scale[:, None]
    return mixed.astype(jnp.bfloat16)


def solution(mesh):
    return jax.shard_map(
        per_device,
        mesh=mesh,
        in_specs=(
            P("sp", ("fs", "tp")),
            P(),
            P(None, ("fs", "tp")),
            P(None, ("fs", "tp")),
            P(None, ("fs", "tp")),
            P(None, ("fs", "tp")),
            P(None, ("fs", "tp")),
            P(),
            P(),
            P(("fs", "tp"), "sp"),
            P(),
            P(),
            P(None, ("fs", "tp")),
        ),
        out_specs=P("sp", ("fs", "tp")),
        check_vma=False,
    )
```

profile of v0, /device:TPU:0, one launch (start us, length us, event | category | flops | bytes accessed | tf_op | source)
XLA Modules:
  0.0 200.8 jit_solution(11392080675907995282)
XLA Ops:
  6.5 0.0 copy-start.2
  6.5 0.0 copy-start.4
  6.5 0.0 all-gather.4.cloned.1.call-start
  6.5 0.7 all-gather.4.cloned.1.call-update
  7.3 0.0 all-gather.8.cloned.1.call-start
  7.3 13.8 %all_gather.22 = bf16[2,2048]{1,0:T(2,128)(2,1)S(1)} all-gather(bf16[2,512]{1,0:T(2,128)(2,1)} %param.24), channel_id=1, replica_groups=mesh['sp'=4,'fs'=4,'tp'=2] {'sp'}, dimensions={1}, use_global_device_ids=true | all-gather | bytes 10240 | tf_op jit(solution)/shard_map/all_gather | solution.py:105
  21.1 1.9 constant_dynamic-update-slice_fusion.4
  23.0 1.9 constant_dynamic-update-slice_fusion.3
  24.9 1.9 constant_dynamic-update-slice_fusion.2
  26.9 1.9 constant_dynamic-update-slice_fusion.1
  28.8 0.0 copy-done.2
  28.8 0.9 constant_dynamic-update-slice_fusion
  29.6 10.4 %all-gather.4.cloned.1.call-done = bf16[512,2048]{1,0:T(8,128)(2,1)} async-done(((bf16[512,256]{1,0:T(8,128)(2,1)}), bf16[512,2048]{1,0:T(8,128)(2,1)}) %all-gather.4.cloned.1.call-update) | async-done | bytes 2097168 | tf_op jit(solution)/shard_map/all_gather | solution.py:41
  40.1 2.1 %fusion.19 = f32[512]{0:T(512)S(1)} fusion(bf16[512,2048]{1,0:T(8,128)(2,1)} %all-gather.4.cloned.1.call-done), kind=kLoop, calls=%fused_computation.37 | loop fusion | flops 3145216 | bytes 2099200 | tf_op jit(solution)/shard_map/reduce_sum | solution.py:45
  42.2 0.0 copy-done.4
  42.2 4.2 %fusion.30 = bf16[512,640]{1,0:T(8,128)(2,1)S(1)} fusion(bf16[2048,640]{1,0:T(8,128)(2,1)} %constant_dynamic-update-slice_fusion, bf16[512,2048]{1,0:T(8,128)(2,1)} %all-gather.4.cloned.1.call-done, f32[2048]{0:T(1024)S(1)} %copy-done.4, f32[512]{0:T(512)S(1)} %add_rsqrt_fusion.3), kind=kOutput, calls=%fused_computation.78 | convolution fusion | flops 1345978368 | bytes 5384192 | tf_op jit(solution)/shard_map/dot_general | solution.py:44
  46.3 0.1 fusion.132
  46.4 16.1 %all_gather.20 = bf16[2048,128]{1,0:T(8,128)(2,1)S(1)} all-gather(bf16[512,128]{1,0:T(8,128)(2,1)S(1)} %get-tuple-element.135), channel_id=1, replica_groups=mesh['sp'=4,'fs'=4,'tp'=2] {'sp'}, dimensions={0}, use_global_device_ids=true | all-gather | bytes 655360 | tf_op jit(solution)/shard_map/all_gather | solution.py:104
  62.5 16.0 %all_gather.21 = bf16[2048,128]{1,0:T(8,128)(2,1)S(1)} all-gather(bf16[512,128]{1,0:T(8,128)(2,1)S(1)} %get-tuple-element.134), channel_id=1, replica_groups=mesh['sp'=4,'fs'=4,'tp'=2] {'sp'}, dimensions={0}, use_global_device_ids=true | all-gather | bytes 655360 | tf_op jit(solution)/shard_map/all_gather | solution.py:103
  78.5 0.1 copy.23
  78.7 0.0 copy-start.5
  78.7 31.2 %while.13 = (s32[]{:T(128)}, f32[512,2,64]{0,2,1:T(8,128)S(1)}, f32[2,512]{1,0:T(2,128)S(1)}, s32[]{:T(128)}, s32[]{:T(128)}, /*index=5*/bf16[2048,128]{1,0:T(8,...) while((s32[]{:T(128)}, f32[512,2,64]{0,2,1:T(8,128)S(1)}, ...), condition=%wide.region_10.11_spmd.clone, body=%wide.region_6.10_spmd.clone.sunk | while | flops 439489024 | bytes 84838688 | solution.py:121
  78.9 0.1 copy.36
  79.2 0.8 compare_and_fusion.2
  80.0 0.1 copy.37
  80.2 5.1 %fusion.152 = (f32[2,512]{1,0:T(2,128)S(1)}, f32[2,512,1024]{1,2,0:T(8,128)S(1)}, f32[2,1024,512]{2,1,0:T(8,128)}) fusion(f32[2,1024]{1,0:T(2,128)S(1)} %dynamic-slice_convert_fusion.3, pred[512,1024]{0,1:T(8,128)(4,1)S(1)} %compare_and_fusion.2, bf16[1024,2,64]{0,2,1:T(8,128)(2,1)S(1)} %bitcast.133, bf16[512,2,64]{0,2,1:T(8,128)(2,1)S(1)} %get-tuple-element.278), kind=kOutput, calls=%fused_computation.33.clone.1 | convolution fusion | flops 145751040 | bytes 9318400 | tf_op jit(solution)/shard_map/while/body/qhd,khd->hqk/dot_general | solution.py:82
  85.2 10.1 %fusion.153 = f32[2,512,8,128]{1,2,3,0:T(8,128)S(1)} fusion(f32[2,512,8,128]{1,3,2,0:T(8,128)S(1)} %bitcast.131), kind=kOutput, calls=%fused_computation.19.clone.1 | output fusion | flops 133169152 | bytes 8388608 | tf_op jit(solution)/shard_map/reduce-window
  95.3 0.0 copy-start
  95.3 2.0 copy-done
  97.3 0.1 reduce-window.16
  97.4 2.7 %broadcast_add_fusion.2 = f32[2,512,8,128]{1,2,3,0:T(8,128)S(1)} fusion(f32[2,512,8,128]{1,2,3,0:T(8,128)} %copy-done, f32[2,512,8]{1,2,0:T(8,128)S(1)} %slice.847), kind=kLoop, calls=%fused_computation.22.clone.1 | loop fusion | flops 1048576 | bytes 8421376 | tf_op jit(solution)/shard_map/reduce_window_sum | solution.py:89
  100.1 0.0 copy-start.1
  100.1 2.4 %copy.38 = f32[2,512,8,128]{1,3,2,0:T(8,128)S(1)} copy(f32[2,512,8,128]{1,2,3,0:T(8,128)S(1)} %broadcast_add_fusion.2) | data formatting | bytes 8388608 | tf_op jit(solution)/shard_map/reduce_window_sum | solution.py:89
  102.5 0.0 copy-done.1
  102.5 6.9 %fusion.154 = bf16[2,512,1024]{1,2,0:T(8,128)(2,1)S(1)} fusion(f32[2,512,8,128]{1,3,2,0:T(8,128)S(1)} %copy.38, f32[2,1024,512]{2,1,0:T(8,128)S(1)} %copy-done.1, f32[2,512]{1,0:T(2,128)S(1)} %get-tuple-element.258, f32[2,1024]{1,0:T(2,128)S(1)} %dynamic-slice_convert_fusion.3, pred[512,1024]{0,1:T(8,128)(4,1)S(1)} %compare_and_fusion.2), kind=kLoop, calls=%fused_computation.7.clone.1 | loop fusion | flops 24117248 | bytes 11022336 | tf_op jit(solution)/shard_map/while/body/convert_element_type | solution.py:90
  109.4 0.5 fusion.155
  109.9 0.0 copy-start.3
  109.9 0.0 copy-start.6
  109.9 0.7 convert_element_type.57
  110.6 0.0 all-gather.8.cloned.1.call-update
  110.6 0.0 all-gather.6.cloned.1.call-start
  110.7 0.7 dynamic-slice_convert_fusion.1
  111.4 0.1 divide_multiply_fusion
  111.5 3.2 %collective-permute-start = (f32[30,128]{1,0:T(8,128)S(1)}, f32[30,128]{1,0:T(8,128)S(1)}, u32[]{:S(2)}, u32[]{:S(2)}) collective-permute-start(f32[30,128]{1,0:T(8,128)S(1)} %slice.285), channel_id=1, source_target_pairs={{0,8},{8,16},{16,24},{1,9},{9,17},{17,25},{2,10},{10,18},{18,26},{... | collective-permute-start | bytes 46088 | tf_op jit(solution)/shard_map/ppermute | solution.py:13
  114.7 0.8 dynamic_slice.19
  115.5 0.4 collective-permute-done
  115.9 1.1 fusion.130
  117.0 11.8 %all-reduce = (f32[512]{0:T(512)S(1)}, f32[512]{0:T(512)S(1)}) all-reduce(f32[512]{0:T(512)S(1)} %get-tuple-element.104, f32[512]{0:T(512)S(1)} %get-tuple-element.103), channel_id=1, replica_groups=mesh['sp'=4,'fs'=4,'tp'=2] {'fs','tp'}, use_global_device_ids=true, to_apply=%region_4.0 | all-reduce | flops 1024 | bytes 8192 | tf_op jit(solution)/shard_map/psum | solution.py:63
  128.8 0.9 multiply_convert_fusion
  129.7 0.0 all-gather.6.cloned.1.call-update
  129.7 35.2 %all-gather.8.cloned.1.call-done = bf16[512,1024]{0,1:T(8,128)(2,1)} async-done(((bf16[512,128]{0,1:T(8,128)(2,1)}), bf16[512,1024]{0,1:T(8,128)(2,1)}) %all-gather.8.cloned.1.call-update) | async-done | bytes 1048592 | tf_op jit(solution)/shard_map/all_gather | solution.py:124
  164.9 1.5 fusion.23
  166.4 0.0 copy-done.5
  166.4 2.0 %convolution_multiply_fusion = f32[512,256]{1,0:T(8,128)S(1)} fusion(bf16[512,1024]{0,1:T(8,128)(2,1)} %all-gather.8.cloned.1.call-done, f32[1024]{0:T(1024)S(1)} %copy-done.5, bf16[2048,256]{1,0:T(8,128)(2,1)} %param.27, f32[512]{0:T(512)S(1)} %add_rsqrt_fusion), kind=kOutput, calls=%fused_computation.79 | convolution fusion | flops 270139392 | bytes 2103296 | tf_op jit(solution)/shard_map/dot_general | solution.py:133
  168.5 21.8 %all-gather.6.cloned.1.call-done = bf16[512,1024]{1,0:T(8,128)(2,1)} async-done(((bf16[512,128]{1,0:T(8,128)(2,1)}), bf16[512,1024]{1,0:T(8,128)(2,1)}) %all-gather.6.cloned.1.call-update) | async-done | bytes 1048592 | tf_op jit(solution)/shard_map/all_gather | solution.py:123
  190.3 1.5 fusion.21
  191.8 0.0 copy-done.3
  191.8 0.0 copy-done.6
  191.8 2.4 %fusion.34 = bf16[512,256]{1,0:T(8,128)(2,1)} fusion(f32[512,256]{1,0:T(8,128)S(1)} %convolution_multiply_fusion, bf16[512,1024]{1,0:T(8,128)(2,1)} %all-gather.6.cloned.1.call-done, f32[1024]{0:T(1024)S(1)} %copy-done.6, bf16[2048,256]{1,0:T(8,128)(2,1)S(1)} %copy-done.3, f32[512]{0:T(512)S(1)} %add_rsqrt_fusion.1), kind=kOutput, calls=%fused_computation.82 | convolution fusion | flops 270401536 | bytes 2365440 | tf_op jit(solution)/shard_map/dot_general | solution.py:132
  (17 shorter events, 0.2 us)
Async XLA Ops:
  6.5 22.2 %copy-start.2 = (bf16[2048,128]{1,0:T(8,128)(2,1)S(1)}, bf16[2048,128]{1,0:T(8,128)(2,1)}, u32[]{:S(2)}) copy-start(bf16[2048,128]{1,0:T(8,128)(2,1)} %param.21) | copy-start | bytes 1572868
  6.5 35.6 %copy-start.4 = (f32[2048]{0:T(1024)S(1)}, f32[2048]{0:T(1024)}, u32[]{:S(2)}) copy-start(f32[2048]{0:T(1024)} %param.16) | copy-start | bytes 24580
  6.5 33.5 %all-gather.4.cloned.1.call-start = ((), (), s32[]{:S(2)}) async-start(), calls=%async_computation | async-start | bytes 2359296 | tf_op jit(solution)/shard_map/all_gather | solution.py:41
  7.3 157.6 %all-gather.8.cloned.1.call-start = ((), (), s32[]{:S(2)}) async-start(), calls=%async_computation.2 | async-start | bytes 1179648 | tf_op jit(solution)/shard_map/all_gather | solution.py:124
  78.7 87.8 %copy-start.5 = (f32[1024]{0:T(1024)S(1)}, f32[1024]{0:T(1024)}, u32[]{:S(2)}) copy-start(f32[1024]{0:T(1024)} %param.26) | copy-start | bytes 12292
  95.3 2.0 copy-start
  100.1 2.4 %copy-start.1 = (f32[2,1024,512]{2,1,0:T(8,128)S(1)}, f32[2,1024,512]{2,1,0:T(8,128)}, u32[]{:S(2)}) copy-start(f32[2,1024,512]{2,1,0:T(8,128)} %get-tuple-element.239) | copy-start | bytes 12582916 | tf_op jit(solution)/shard_map/while
  109.9 81.9 %copy-start.3 = (bf16[2048,256]{1,0:T(8,128)(2,1)S(1)}, bf16[2048,256]{1,0:T(8,128)(2,1)}, u32[]{:S(2)}) copy-start(bf16[2048,256]{1,0:T(8,128)(2,1)} %param.27) | copy-start | bytes 3145732
  109.9 81.9 %copy-start.6 = (f32[1024]{0:T(1024)S(1)}, f32[1024]{0:T(1024)}, u32[]{:S(2)}) copy-start(f32[1024]{0:T(1024)} %param.25) | copy-start | bytes 12292
  110.6 79.7 %all-gather.6.cloned.1.call-start = ((), (), s32[]{:S(2)}) async-start(), calls=%async_computation.1 | async-start | bytes 1179648 | tf_op jit(solution)/shard_map/all_gather | solution.py:123
  111.5 4.4 %collective-permute-start = (f32[30,128]{1,0:T(8,128)S(1)}, f32[30,128]{1,0:T(8,128)S(1)}, u32[]{:S(2)}, u32[]{:S(2)}) collective-permute-start(f32[30,128]{1,0:T(8,128)S(1)} %slice.285), channel_id=1, source_target_pairs={{0,8},{8,16},{16,24},{1,9},{9,17},{17,25},{2,10},{10,18},{18,26},{... | collective-permute-start | bytes 46088 | tf_op jit(solution)/shard_map/ppermute | solution.py:13
Sparse Core Ops, SparseCore 0:
  9.2 30.8 all-gather.3
  110.7 54.1 all-gather.7
  166.8 23.4 all-gather.5
where the time goes:
time: 201 us
  waiting for transfers between devices  68.6 us (34%)
  blocking collectives  57.7 us (29%)
  other arithmetic  29.1 us (14%)
  local copies, waits for them, and re-layouts  14.3 us (7%)
  matrix products  14.1 us (7%)
  between operations  13.3 us (7%)
  starting transfers between devices  3.27 us (2%)
    all_gather x1, waiting for transfers between devices, per_device(): attn_piece = lax.all_gather(attn_mixed, ('fs', 'tp'), axis=1, tiled=True)  35.2 us
    all_gather x1, waiting for transfers between devices, per_device(): conv_piece = lax.all_gather(conv_mixed, ('fs', 'tp'), axis=1, tiled=True)  21.8 us
    all_gather x1, blocking collectives, per_device(): lax.all_gather(value, 'sp', axis=0, tiled=True)  16.1 us
    all_gather x1, blocking collectives, per_device(): lax.all_gather(key, 'sp', axis=0, tiled=True)  16 us
    all_gather x1, blocking collectives, per_device(): lax.all_gather(break_shift, 'sp', axis=1, tiled=True)  13.8 us
    psum x1, blocking collectives, per_device(): lax.psum((jnp.sum(conv_out, axis=1), jnp.sum(conv_out * conv_out, axis=1)...  11.8 us
    all_gather x1, waiting for transfers between devices, per_device(): segment = lax.all_gather(tokens, ('fs', 'tp'), axis=1, tiled=True)  10.4 us
    another operation x2, other arithmetic  10.1 us
  transfers between devices with their start and end apart: 4, of which 4 were waited for; matrix products, arithmetic and copies ran while one was open for 8% of the time, Pallas kernels for 0%

commit v1 on v0

--- a/solution.py
+++ b/solution.py
@@ -61,7 +61,7 @@
     for offset in range(reach_rows + 1):
         conv_out = conv_out + tap_values[offset][None, :] * padded[offset : offset + rows_here]
     first_sum, second_sum = lax.psum(
-        (jnp.sum(conv_out, axis=1), jnp.sum(conv_out * conv_out, axis=1)), ("fs", "tp")
+        lax.psum((jnp.sum(conv_out, axis=1), jnp.sum(conv_out * conv_out, axis=1)), "tp"), "fs"
     )
     row_mean = first_sum / channels
     row_spread = second_sum / channels - row_mean * row_mean

time: 201 us -> 201 us (level)
    psum x1, blocking collectives: 11.8 us -> 2.47 us  [per_device(): lax.psum((jnp.sum(conv_out, axis=1), jnp.sum(conv_out * conv_out, axis=1)...]
    psum x0 -> x1, blocking collectives: none -> 8.91 us  [per_device(): lax.psum(lax.psum((jnp.sum(conv_out, axis=1), jnp.sum(conv_out * conv_out...]
where the time goes in v1:
time: 201 us
  waiting for transfers between devices  69.1 us (34%)
  blocking collectives  57.2 us (28%)
  other arithmetic  29.1 us (14%)
  local copies, waits for them, and re-layouts  14.3 us (7%)
  matrix products  14.1 us (7%)
  between operations  13.3 us (7%)
  starting transfers between devices  3.27 us (2%)
    all_gather x1, waiting for transfers between devices, per_device(): attn_piece = lax.all_gather(attn_mixed, ('fs', 'tp'), axis=1, tiled=True)  35.6 us
    all_gather x1, waiting for transfers between devices, per_device(): conv_piece = lax.all_gather(conv_mixed, ('fs', 'tp'), axis=1, tiled=True)  21.8 us
    all_gather x1, blocking collectives, per_device(): lax.all_gather(value, 'sp', axis=0, tiled=True)  16.1 us
    all_gather x1, blocking collectives, per_device(): lax.all_gather(key, 'sp', axis=0, tiled=True)  16 us
    all_gather x1, blocking collectives, per_device(): lax.all_gather(break_shift, 'sp', axis=1, tiled=True)  13.8 us
    all_gather x1, waiting for transfers between devices, per_device(): segment = lax.all_gather(tokens, ('fs', 'tp'), axis=1, tiled=True)  10.4 us
    another operation x2, other arithmetic  10.1 us
    psum x1, blocking collectives, per_device(): lax.psum(lax.psum((jnp.sum(conv_out, axis=1), jnp.sum(conv_out * conv_out...  8.91 us
  transfers between devices with their start and end apart: 4, of which 4 were waited for; matrix products, arithmetic and copies ran while one was open for 8% of the time, Pallas kernels for 0%

profile of v1, /device:TPU:0, one launch (start us, length us, event | category | flops | bytes accessed | tf_op | source)
XLA Modules:
  0.0 200.7 jit_solution(5882551026464136704)
XLA Ops:
  6.5 0.0 copy-start.2
  6.5 0.0 copy-start.4
  6.5 0.0 all-gather.4.cloned.1.call-start
  6.5 0.7 all-gather.4.cloned.1.call-update
  7.3 0.0 all-gather.8.cloned.1.call-start
  7.3 13.8 %all_gather.22 = bf16[2,2048]{1,0:T(2,128)(2,1)S(1)} all-gather(bf16[2,512]{1,0:T(2,128)(2,1)} %param.24), channel_id=1, replica_groups=mesh['sp'=4,'fs'=4,'tp'=2] {'sp'}, dimensions={1}, use_global_device_ids=true | all-gather | bytes 10240 | tf_op jit(solution)/shard_map/all_gather | solution.py:105
  21.1 1.9 constant_dynamic-update-slice_fusion.4
  23.0 1.9 constant_dynamic-update-slice_fusion.3
  24.9 1.9 constant_dynamic-update-slice_fusion.2
  26.9 1.9 constant_dynamic-update-slice_fusion.1
  28.8 0.0 copy-done.2
  28.8 0.9 constant_dynamic-update-slice_fusion
  29.6 10.4 %all-gather.4.cloned.1.call-done = bf16[512,2048]{1,0:T(8,128)(2,1)} async-done(((bf16[512,256]{1,0:T(8,128)(2,1)}), bf16[512,2048]{1,0:T(8,128)(2,1)}) %all-gather.4.cloned.1.call-update) | async-done | bytes 2097168 | tf_op jit(solution)/shard_map/all_gather | solution.py:41
  40.1 2.1 %fusion.19 = f32[512]{0:T(512)S(1)} fusion(bf16[512,2048]{1,0:T(8,128)(2,1)} %all-gather.4.cloned.1.call-done), kind=kLoop, calls=%fused_computation.37 | loop fusion | flops 3145216 | bytes 2099200 | tf_op jit(solution)/shard_map/reduce_sum | solution.py:45
  42.2 0.0 copy-done.4
  42.2 4.2 %fusion.30 = bf16[512,640]{1,0:T(8,128)(2,1)S(1)} fusion(bf16[2048,640]{1,0:T(8,128)(2,1)} %constant_dynamic-update-slice_fusion, bf16[512,2048]{1,0:T(8,128)(2,1)} %all-gather.4.cloned.1.call-done, f32[2048]{0:T(1024)S(1)} %copy-done.4, f32[512]{0:T(512)S(1)} %add_rsqrt_fusion.3), kind=kOutput, calls=%fused_computation.78 | convolution fusion | flops 1345978368 | bytes 5384192 | tf_op jit(solution)/shard_map/dot_general | solution.py:44
  46.3 0.1 fusion.132
  46.4 16.1 %all_gather.20 = bf16[2048,128]{1,0:T(8,128)(2,1)S(1)} all-gather(bf16[512,128]{1,0:T(8,128)(2,1)S(1)} %get-tuple-element.137), channel_id=1, replica_groups=mesh['sp'=4,'fs'=4,'tp'=2] {'sp'}, dimensions={0}, use_global_device_ids=true | all-gather | bytes 655360 | tf_op jit(solution)/shard_map/all_gather | solution.py:104
  62.5 16.0 %all_gather.21 = bf16[2048,128]{1,0:T(8,128)(2,1)S(1)} all-gather(bf16[512,128]{1,0:T(8,128)(2,1)S(1)} %get-tuple-element.136), channel_id=1, replica_groups=mesh['sp'=4,'fs'=4,'tp'=2] {'sp'}, dimensions={0}, use_global_device_ids=true | all-gather | bytes 655360 | tf_op jit(solution)/shard_map/all_gather | solution.py:103
  78.5 0.1 copy.23
  78.7 0.0 copy-start.5
  78.7 31.2 %while.13 = (s32[]{:T(128)}, f32[512,2,64]{0,2,1:T(8,128)S(1)}, f32[2,512]{1,0:T(2,128)S(1)}, s32[]{:T(128)}, s32[]{:T(128)}, /*index=5*/bf16[2048,128]{1,0:T(8,...) while((s32[]{:T(128)}, f32[512,2,64]{0,2,1:T(8,128)S(1)}, ...), condition=%wide.region_12.13_spmd.clone, body=%wide.region_8.12_spmd.clone.sunk | while | flops 439489024 | bytes 84838688 | solution.py:121
  78.9 0.1 copy.36
  79.2 0.8 compare_and_fusion.2
  80.0 0.1 copy.37
  80.2 5.1 %fusion.152 = (f32[2,512]{1,0:T(2,128)S(1)}, f32[2,512,1024]{1,2,0:T(8,128)S(1)}, f32[2,1024,512]{2,1,0:T(8,128)}) fusion(f32[2,1024]{1,0:T(2,128)S(1)} %dynamic-slice_convert_fusion.3, pred[512,1024]{0,1:T(8,128)(4,1)S(1)} %compare_and_fusion.2, bf16[1024,2,64]{0,2,1:T(8,128)(2,1)S(1)} %bitcast.133, bf16[512,2,64]{0,2,1:T(8,128)(2,1)S(1)} %get-tuple-element.280), kind=kOutput, calls=%fused_computation.33.clone.1 | convolution fusion | flops 145751040 | bytes 9318400 | tf_op jit(solution)/shard_map/while/body/qhd,khd->hqk/dot_general | solution.py:82
  85.2 10.1 %fusion.153 = f32[2,512,8,128]{1,2,3,0:T(8,128)S(1)} fusion(f32[2,512,8,128]{1,3,2,0:T(8,128)S(1)} %bitcast.131), kind=kOutput, calls=%fused_computation.19.clone.1 | output fusion | flops 133169152 | bytes 8388608 | tf_op jit(solution)/shard_map/reduce-window
  95.3 0.0 copy-start
  95.3 2.0 copy-done
  97.3 0.1 reduce-window.16
  97.4 2.7 %broadcast_add_fusion.2 = f32[2,512,8,128]{1,2,3,0:T(8,128)S(1)} fusion(f32[2,512,8,128]{1,2,3,0:T(8,128)} %copy-done, f32[2,512,8]{1,2,0:T(8,128)S(1)} %slice.847), kind=kLoop, calls=%fused_computation.22.clone.1 | loop fusion | flops 1048576 | bytes 8421376 | tf_op jit(solution)/shard_map/reduce_window_sum | solution.py:89
  100.1 0.0 copy-start.1
  100.1 2.4 %copy.38 = f32[2,512,8,128]{1,3,2,0:T(8,128)S(1)} copy(f32[2,512,8,128]{1,2,3,0:T(8,128)S(1)} %broadcast_add_fusion.2) | data formatting | bytes 8388608 | tf_op jit(solution)/shard_map/reduce_window_sum | solution.py:89
  102.5 0.0 copy-done.1
  102.5 6.9 %fusion.154 = bf16[2,512,1024]{1,2,0:T(8,128)(2,1)S(1)} fusion(f32[2,512,8,128]{1,3,2,0:T(8,128)S(1)} %copy.38, f32[2,1024,512]{2,1,0:T(8,128)S(1)} %copy-done.1, f32[2,512]{1,0:T(2,128)S(1)} %get-tuple-element.260, f32[2,1024]{1,0:T(2,128)S(1)} %dynamic-slice_convert_fusion.3, pred[512,1024]{0,1:T(8,128)(4,1)S(1)} %compare_and_fusion.2), kind=kLoop, calls=%fused_computation.7.clone.1 | loop fusion | flops 24117248 | bytes 11022336 | tf_op jit(solution)/shard_map/while/body/convert_element_type | solution.py:90
  109.4 0.5 fusion.155
  109.9 0.0 copy-start.3
  109.9 0.0 copy-start.6
  109.9 0.7 convert_element_type.57
  110.6 0.0 all-gather.8.cloned.1.call-update
  110.6 0.0 all-gather.6.cloned.1.call-start
  110.7 0.7 dynamic-slice_convert_fusion.1
  111.4 0.1 divide_multiply_fusion
  111.5 3.2 %collective-permute-start = (f32[30,128]{1,0:T(8,128)S(1)}, f32[30,128]{1,0:T(8,128)S(1)}, u32[]{:S(2)}, u32[]{:S(2)}) collective-permute-start(f32[30,128]{1,0:T(8,128)S(1)} %slice.285), channel_id=1, source_target_pairs={{0,8},{8,16},{16,24},{1,9},{9,17},{17,25},{2,10},{10,18},{18,26},{... | collective-permute-start | bytes 46088 | tf_op jit(solution)/shard_map/ppermute | solution.py:13
  114.7 0.8 dynamic_slice.19
  115.5 0.4 collective-permute-done
  115.9 1.1 fusion.130
  117.0 2.5 %all-reduce.1 = (f32[512]{0:T(512)S(1)}, f32[512]{0:T(512)S(1)}) all-reduce(f32[512]{0:T(512)S(1)} %get-tuple-element.104, f32[512]{0:T(512)S(1)} %get-tuple-element.103), channel_id=1, replica_groups=mesh['sp'=4,'fs'=4,'tp'=2] {'tp'}, use_global_device_ids=true, to_apply=%region_5.0 | all-reduce | flops 1024 | bytes 8192 | tf_op jit(solution)/shard_map/psum | solution.py:64
  119.4 8.9 %all-reduce = (f32[512]{0:T(512)S(1)}, f32[512]{0:T(512)S(1)}) all-reduce(f32[512]{0:T(512)S(1)} %get-tuple-element.127, f32[512]{0:T(512)S(1)} %get-tuple-element.128), channel_id=1, replica_groups=mesh['sp'=4,'fs'=4,'tp'=2] {'fs'}, use_global_device_ids=true, to_apply=%region_6.0 | all-reduce | flops 1024 | bytes 8192 | tf_op jit(solution)/shard_map/psum | solution.py:63
  128.4 0.9 multiply_convert_fusion
  129.2 0.0 all-gather.6.cloned.1.call-update
  129.3 35.6 %all-gather.8.cloned.1.call-done = bf16[512,1024]{0,1:T(8,128)(2,1)} async-done(((bf16[512,128]{0,1:T(8,128)(2,1)}), bf16[512,1024]{0,1:T(8,128)(2,1)}) %all-gather.8.cloned.1.call-update) | async-done | bytes 1048592 | tf_op jit(solution)/shard_map/all_gather | solution.py:124
  164.9 1.5 fusion.23
  166.4 0.0 copy-done.5
  166.4 2.0 %convolution_multiply_fusion = f32[512,256]{1,0:T(8,128)S(1)} fusion(bf16[512,1024]{0,1:T(8,128)(2,1)} %all-gather.8.cloned.1.call-done, f32[1024]{0:T(1024)S(1)} %copy-done.5, bf16[2048,256]{1,0:T(8,128)(2,1)} %param.27, f32[512]{0:T(512)S(1)} %add_rsqrt_fusion), kind=kOutput, calls=%fused_computation.79 | convolution fusion | flops 270139392 | bytes 2103296 | tf_op jit(solution)/shard_map/dot_general | solution.py:133
  168.5 21.8 %all-gather.6.cloned.1.call-done = bf16[512,1024]{1,0:T(8,128)(2,1)} async-done(((bf16[512,128]{1,0:T(8,128)(2,1)}), bf16[512,1024]{1,0:T(8,128)(2,1)}) %all-gather.6.cloned.1.call-update) | async-done | bytes 1048592 | tf_op jit(solution)/shard_map/all_gather | solution.py:123
  190.3 1.5 fusion.21
  191.8 0.0 copy-done.3
  191.8 0.0 copy-done.6
  191.8 2.4 %fusion.34 = bf16[512,256]{1,0:T(8,128)(2,1)} fusion(f32[512,256]{1,0:T(8,128)S(1)} %convolution_multiply_fusion, bf16[512,1024]{1,0:T(8,128)(2,1)} %all-gather.6.cloned.1.call-done, f32[1024]{0:T(1024)S(1)} %copy-done.6, bf16[2048,256]{1,0:T(8,128)(2,1)S(1)} %copy-done.3, f32[512]{0:T(512)S(1)} %add_rsqrt_fusion.1), kind=kOutput, calls=%fused_computation.82 | convolution fusion | flops 270401536 | bytes 2365440 | tf_op jit(solution)/shard_map/dot_general | solution.py:132
  (17 shorter events, 0.2 us)
Async XLA Ops:
  6.5 22.2 %copy-start.2 = (bf16[2048,128]{1,0:T(8,128)(2,1)S(1)}, bf16[2048,128]{1,0:T(8,128)(2,1)}, u32[]{:S(2)}) copy-start(bf16[2048,128]{1,0:T(8,128)(2,1)} %param.21) | copy-start | bytes 1572868
  6.5 35.6 %copy-start.4 = (f32[2048]{0:T(1024)S(1)}, f32[2048]{0:T(1024)}, u32[]{:S(2)}) copy-start(f32[2048]{0:T(1024)} %param.16) | copy-start | bytes 24580
  6.5 33.5 %all-gather.4.cloned.1.call-start = ((), (), s32[]{:S(2)}) async-start(), calls=%async_computation | async-start | bytes 2359296 | tf_op jit(solution)/shard_map/all_gather | solution.py:41
  7.3 157.6 %all-gather.8.cloned.1.call-start = ((), (), s32[]{:S(2)}) async-start(), calls=%async_computation.2 | async-start | bytes 1179648 | tf_op jit(solution)/shard_map/all_gather | solution.py:124
  78.7 87.7 %copy-start.5 = (f32[1024]{0:T(1024)S(1)}, f32[1024]{0:T(1024)}, u32[]{:S(2)}) copy-start(f32[1024]{0:T(1024)} %param.26) | copy-start | bytes 12292
  95.3 2.0 copy-start
  100.1 2.4 %copy-start.1 = (f32[2,1024,512]{2,1,0:T(8,128)S(1)}, f32[2,1024,512]{2,1,0:T(8,128)}, u32[]{:S(2)}) copy-start(f32[2,1024,512]{2,1,0:T(8,128)} %get-tuple-element.241) | copy-start | bytes 12582916 | tf_op jit(solution)/shard_map/while
  109.9 81.9 %copy-start.3 = (bf16[2048,256]{1,0:T(8,128)(2,1)S(1)}, bf16[2048,256]{1,0:T(8,128)(2,1)}, u32[]{:S(2)}) copy-start(bf16[2048,256]{1,0:T(8,128)(2,1)} %param.27) | copy-start | bytes 3145732
  109.9 81.9 %copy-start.6 = (f32[1024]{0:T(1024)S(1)}, f32[1024]{0:T(1024)}, u32[]{:S(2)}) copy-start(f32[1024]{0:T(1024)} %param.25) | copy-start | bytes 12292
  110.6 79.7 %all-gather.6.cloned.1.call-start = ((), (), s32[]{:S(2)}) async-start(), calls=%async_computation.1 | async-start | bytes 1179648 | tf_op jit(solution)/shard_map/all_gather | solution.py:123
  111.5 4.4 %collective-permute-start = (f32[30,128]{1,0:T(8,128)S(1)}, f32[30,128]{1,0:T(8,128)S(1)}, u32[]{:S(2)}, u32[]{:S(2)}) collective-permute-start(f32[30,128]{1,0:T(8,128)S(1)} %slice.285), channel_id=1, source_target_pairs={{0,8},{8,16},{16,24},{1,9},{9,17},{17,25},{2,10},{10,18},{18,26},{... | collective-permute-start | bytes 46088 | tf_op jit(solution)/shard_map/ppermute | solution.py:13
Sparse Core Ops, SparseCore 0:
  9.2 30.8 all-gather.3
  110.7 54.1 all-gather.7
  166.8 23.4 all-gather.5
